TPU v7x, 512 devices: a whole 4x4x16 slice. The times are simulated.
512 devices in a mesh: sp: 16 (over z), fs: 4 (over y), tp: 8 (over x, core).
Axes of the slice: x: 4, y: 4, z: 16, core: 2. Of those that a mesh axis runs over, the one named last changes fastest.
Arguments:
- tokens: bfloat16 [4, 16384, 2048], P('fs', ('sp', 'tp')), may hold values from -6 to 6
- input_norm_gain: float32 [2048], replicated, may hold values from 0.1 to 1.9
- earlier_gate: bfloat16 [2048, 1024], P(('sp', 'fs'), 'tp'), may hold values from -0.125 to 0.125
- later_gate: bfloat16 [2048, 1024], P(('sp', 'fs'), 'tp'), may hold values from -0.125 to 0.125
- convolution_input: bfloat16 [2048, 1024], P(('sp', 'fs'), 'tp'), may hold values from -0.125 to 0.125
- convolution_taps: float32 [3, 1024], P(None, 'tp'), may hold values from -3 to 3
- receptance: bfloat16 [2048, 1024], P(('sp', 'fs'), 'tp'), may hold values from -0.125 to 0.125
- key_matrix: bfloat16 [2048, 1024], P(('sp', 'fs'), 'tp'), may hold values from -0.125 to 0.125
- value_matrix: bfloat16 [2048, 1024], P(('sp', 'fs'), 'tp'), may hold values from -0.125 to 0.125
- decay_matrix: bfloat16 [2048, 1024], P(('sp', 'fs'), 'tp'), may hold values from -0.125 to 0.125
- rate_matrix: bfloat16 [2048, 1024], P(('sp', 'fs'), 'tp'), may hold values from -0.125 to 0.125
- decay_floor: float32 [1024], P('tp'), may hold values from -16 to -3.4
- rate_offset: float32 [1024], P('tp'), may hold values from -7.5 to 1
- decay_spike: float32 [4, 16384, 1024], P('fs', 'sp', 'tp'), may hold values from -1.3 to 0
- initial_state: float32 [4, 16, 64, 64], P('fs', 'tp'), may hold values from -768 to 768
- head_norm_gain: float32 [1024], P('tp'), may hold values from 0.1 to 1.9
- convolution_output: bfloat16 [1024, 2048], P('tp', ('sp', 'fs')), may hold values from -0.125 to 0.125
- state_heads_output: bfloat16 [1024, 2048], P('tp', ('sp', 'fs')), may hold values from -0.125 to 0.125
Outputs:
- mixed: bfloat16 [4, 16384, 2048], P('fs', ('sp', 'tp'))
All inputs are finite; a program needn't handle non-finite values.
Results may differ from a plain program's by a relative error of at most 0.02.
Values may be sent and summed in bfloat16 or wider, within the bound.
No kernel may reach another device: no remote copies, remote signals or barrier semaphores. Data moves between devices by JAX's collectives and lax.ppermute only.
A program may use at most 64 MiB of HBM per device.

v0:
```python
import jax
import jax.numpy as jnp
from jax import lax
from jax.sharding import PartitionSpec as P

HEAD_WIDTH = 64
BLOCK = 64
norm_eps = 1e-06
key_eps = 1e-06


def passed_along(block, axis, distance):
    devices = range(lax.axis_size(axis))
    route = [(i - distance, i) for i in devices if i - distance in devices]
    return lax.ppermute(block, axis, route)


def side_by_side(arrays, axis, dim, along):
    widths = [a.shape[along] for a in arrays]
    both = jnp.concatenate(arrays, axis=along)
    out = lax.all_gather(both, axis, axis=dim, tiled=True)
    return tuple(jnp.split(out, [sum(widths[:k]) for k in range(1, len(widths))], axis=along))


def from_everyone(x, axis):
    devices = lax.axis_size(axis)
    return lax.all_to_all(jnp.broadcast_to(x[None], (devices, *x.shape)), axis, 0, 0, tiled=True)


def collected_together(x, axis):
    leaves = jax.tree.leaves(x)
    order = sorted(range(len(leaves)), key=lambda k: -leaves[k].size)
    width = (1, *leaves[order[0]].shape)[-1]
    lines = [
        jnp.pad(leaves[k].reshape(-1), (0, -leaves[k].size % width)).reshape(-1, width)
        for k in order
    ]
    both, at, found = (from_everyone(jnp.concatenate(lines), axis), 0, {})
    for k, line in zip(order, lines):
        piece = both[:, at : at + len(line)].reshape(len(both), -1)
        found[k] = piece[:, : leaves[k].size].reshape(-1, *leaves[k].shape)
        at += len(line)
    numbers = iter(range(len(leaves)))
    return jax.tree.map(lambda _: found[next(numbers)], x)


def combined_pairwise(pieces, combine):
    while len(jax.tree.leaves(pieces)[0]) > 1:
        pieces = jax.vmap(combine)(
            *(jax.tree.map(lambda part: part[side::2], pieces) for side in (0, 1))
        )
    return jax.tree.map(lambda part: part[0], pieces)


def entering(x, axis, combine, identity):
    devices, position = (lax.axis_size(axis), lax.axis_index(axis))
    passed = jnp.arange(devices) < position

    def kept(part, zero, own):
        part = jnp.where(
            passed.reshape(-1, *(1 for _ in own.shape)),
            part.astype(own.dtype),
            jnp.asarray(zero, own.dtype),
        )
        return part

    pieces = collected_together(
        jax.tree.map(lambda part, kind: part.astype(kind), x, (jnp.bfloat16, jnp.bfloat16)), axis
    )
    return combined_pairwise(jax.tree.map(kept, pieces, identity, x), combine)


def gather_turned(arrays, axis, dims):
    turned = [jnp.moveaxis(a, dim, 0) for a, dim in zip(arrays, dims)]
    both = jnp.concatenate([t.reshape(len(t), -1) for t in turned], axis=1)
    out, at, outs = (lax.all_gather(both, axis, axis=0, tiled=True), 0, [])
    for t, dim in zip(turned, dims):
        piece = out[:, at : at + t[0].size].reshape(-1, *t.shape[1:])
        outs.append(jnp.moveaxis(piece, 0, dim))
        at += t[0].size
    return tuple(outs)


def rms_rows(activations, gain_vector):
    values = activations.astype(jnp.float32)
    inv_scale = lax.rsqrt(jnp.mean(values * values, axis=-1, keepdims=True) + norm_eps)
    return (values * inv_scale * gain_vector).astype(jnp.bfloat16)


def project(activations, weight):
    return jnp.dot(activations, weight, preferred_element_type=jnp.float32).astype(jnp.bfloat16)


def conv_branch(pre_values, post_values, conv_values, convolution_taps):
    product = pre_values.astype(jnp.float32) * conv_values.astype(jnp.float32)
    reach_rows = convolution_taps.shape[0] - 1
    sequence_rows = product.shape[0]
    edge_rows = passed_along(product[sequence_rows - reach_rows :], "sp", 1)
    padded = jnp.concatenate([edge_rows, product], axis=0)
    filtered = convolution_taps[0] * padded[0:sequence_rows]
    for offset in range(1, convolution_taps.shape[0]):
        filtered = filtered + convolution_taps[offset] * padded[offset : offset + sequence_rows]
    return (post_values.astype(jnp.float32) * filtered).astype(jnp.bfloat16)


def pairs(left_side, right_side, allowed):
    return jnp.where(allowed, jnp.einsum("thj,shj->hts", left_side, right_side), 0.0)


def block_pass(carried, inputs):
    queries, key_rows, value_rows, unit_keys, beta_rows, logarithm_decay = inputs
    span_rows = logarithm_decay.shape[0]
    cumulative = jnp.cumsum(logarithm_decay, axis=0)
    previous = cumulative - logarithm_decay
    middle = cumulative[span_rows // 2]
    later_index = lax.broadcasted_iota(jnp.int32, (span_rows, span_rows), 0)
    earlier_index = lax.broadcasted_iota(jnp.int32, (span_rows, span_rows), 1)
    strict = (later_index > earlier_index)[None]
    inclusive = (later_index >= earlier_index)[None]
    ask_keys = unit_keys * jnp.exp(previous - middle)
    ask_reads = queries * jnp.exp(cumulative - middle)
    give_keys = key_rows * jnp.exp(middle - cumulative)
    give_betas = beta_rows * jnp.exp(middle - cumulative)
    key_ask = pairs(ask_keys, give_keys, strict)
    beta_ask = pairs(ask_keys, give_betas, strict)
    key_read = pairs(ask_reads, give_keys, inclusive)
    beta_read = pairs(ask_reads, give_betas, inclusive)
    extended = jnp.concatenate([value_rows, jnp.zeros_like(value_rows)], axis=2)
    from_start = jnp.einsum("thj,hrj->htr", unit_keys * jnp.exp(previous), carried)
    right_side = from_start + jnp.einsum("hts,shr->htr", key_ask, extended)
    system = beta_ask + jnp.eye(span_rows, dtype=jnp.float32)[None]
    removed = jax.scipy.linalg.solve_triangular(system, right_side, lower=True, unit_diagonal=True)
    outputs = (
        jnp.einsum("thj,hrj->thr", queries * jnp.exp(cumulative), carried)
        + jnp.einsum("hts,shr->thr", key_read, extended)
        - jnp.einsum("hts,hsr->thr", beta_read, removed)
    )
    closing = cumulative[span_rows - 1]
    tail_decay = jnp.exp(closing - cumulative)
    carried = (
        carried * jnp.exp(closing)[:, None, :]
        + jnp.einsum("shr,shj->hrj", extended, key_rows * tail_decay)
        - jnp.einsum("hsr,shj->hrj", removed, beta_rows * tail_decay)
    )
    return (carried, outputs)


def compose(earlier, later):
    return (
        jnp.einsum("hij,hjk->hik", earlier[0], later[0]),
        jnp.einsum("hij,hjk->hik", earlier[1], later[0]) + later[1],
    )


def on_device(
    tokens,
    input_norm_gain,
    earlier_gate,
    later_gate,
    convolution_input,
    convolution_taps,
    receptance,
    key_matrix,
    value_matrix,
    decay_matrix,
    rate_matrix,
    decay_floor,
    rate_offset,
    decay_spike,
    initial_state,
    head_norm_gain,
    convolution_output,
    state_heads_output,
):
    normed = rms_rows(tokens[0], input_norm_gain)
    channels = earlier_gate.shape[1]
    gathered = side_by_side(
        (
            earlier_gate,
            later_gate,
            convolution_input,
            receptance,
            key_matrix,
            value_matrix,
            decay_matrix,
            rate_matrix,
        ),
        ("sp", "fs"),
        0,
        1,
    )
    piece = lax.all_gather(normed, "tp", axis=0, tiled=True)
    projected = jnp.concatenate([project(piece, weight) for weight in gathered], axis=1)
    pieces = jnp.split(projected, 8, axis=1)
    conv_mixed = conv_branch(pieces[0], pieces[1], pieces[2], convolution_taps)
    queries_raw, keys_raw, values_raw, decay_pre, rate_pre = pieces[3:]
    sequence_rows = queries_raw.shape[0]
    present_heads = channels // HEAD_WIDTH

    def by_heads(array):
        return array.astype(jnp.float32).reshape(sequence_rows, present_heads, HEAD_WIDTH)

    queries = by_heads(queries_raw)
    key_rows = by_heads(keys_raw)
    value_rows = by_heads(values_raw)
    logarithm_decay = -jnp.exp(
        decay_floor.reshape(present_heads, HEAD_WIDTH) + jnp.tanh(by_heads(decay_pre))
    )
    logarithm_decay = logarithm_decay + decay_spike[0].reshape(
        sequence_rows, present_heads, HEAD_WIDTH
    )
    learn_rate = jax.nn.sigmoid(rate_offset.reshape(present_heads, HEAD_WIDTH) + by_heads(rate_pre))
    unit_keys = key_rows * lax.rsqrt(jnp.sum(key_rows * key_rows, axis=-1, keepdims=True) + key_eps)
    beta_rows = learn_rate * unit_keys
    blocks = sequence_rows // BLOCK

    def in_blocks(array):
        return array.reshape(blocks, BLOCK, present_heads, HEAD_WIDTH)

    identity = jnp.broadcast_to(
        jnp.eye(HEAD_WIDTH, dtype=jnp.float32), (present_heads, HEAD_WIDTH, HEAD_WIDTH)
    )
    initial_rows = jnp.concatenate(
        [jnp.zeros((present_heads, HEAD_WIDTH, HEAD_WIDTH), jnp.float32), identity], axis=1
    )
    ending, outputs = lax.scan(
        block_pass,
        initial_rows,
        tuple(
            (
                in_blocks(array)
                for array in (queries, key_rows, value_rows, unit_keys, beta_rows, logarithm_decay)
            )
        ),
    )
    outputs = outputs.reshape(sequence_rows, present_heads, 2 * HEAD_WIDTH)
    carry_source = ending[:, :HEAD_WIDTH, :]
    carry_map = ending[:, HEAD_WIDTH:, :]
    first_state = initial_state[0]
    prefix_map, prefix_source = entering(
        (carry_map, carry_source), "sp", compose, (identity, jnp.zeros_like(carry_source))
    )
    opening_state = jnp.einsum("hvj,hjk->hvk", first_state, prefix_map) + prefix_source
    reads = outputs[..., :HEAD_WIDTH] + jnp.einsum(
        "thj,hvj->thv", outputs[..., HEAD_WIDTH:], opening_state
    )
    centered = reads - jnp.mean(reads, axis=-1, keepdims=True)
    variance = jnp.mean(centered * centered, axis=-1, keepdims=True)
    state_mixed = (
        centered
        * lax.rsqrt(variance + HEAD_WIDTH * 1e-05)
        * head_norm_gain.reshape(present_heads, HEAD_WIDTH)
    )
    state_mixed = state_mixed.reshape(sequence_rows, channels).astype(jnp.bfloat16)
    conv_whole, state_whole = gather_turned(
        (convolution_output, state_heads_output), ("sp", "fs"), (1, 1)
    )
    mixed = lax.psum_scatter(
        (
            jnp.dot(conv_mixed, conv_whole, preferred_element_type=jnp.float32)
            + jnp.dot(state_mixed, state_whole, preferred_element_type=jnp.float32)
        ).astype(jnp.bfloat16),
        "tp",
        scatter_dimension=0,
        tiled=True,
    )
    return mixed[None]


def solution(mesh):
    placed = (
        P("fs", ("sp", "tp"), None),
        P(),
        P(("sp", "fs"), "tp"),
        P(("sp", "fs"), "tp"),
        P(("sp", "fs"), "tp"),
        P(None, "tp"),
        P(("sp", "fs"), "tp"),
        P(("sp", "fs"), "tp"),
        P(("sp", "fs"), "tp"),
        P(("sp", "fs"), "tp"),
        P(("sp", "fs"), "tp"),
        P("tp"),
        P("tp"),
        P("fs", "sp", "tp"),
        P("fs", "tp", None, None),
        P("tp"),
        P("tp", ("sp", "fs")),
        P("tp", ("sp", "fs")),
    )
    return jax.shard_map(
        on_device,
        mesh=mesh,
        in_specs=placed,
        out_specs=P("fs", ("sp", "tp"), None),
        check_vma=False,
    )
```

profile of v0, /device:TPU:8, one launch (start us, length us, event | category | flops | bytes accessed | tf_op | source)
XLA Modules:
  0.0 573.6 jit_solution(10139626129675810700)
XLA Ops:
  6.5 1.3 fusion.63
  7.8 2.0 fusion.65
  16.2 1.3 pad_maximum_fusion.2
  18.3 2.6 reshape_squeeze.3
  21.9 32.2 %all-gather.4.cloned.1.call-done = bf16[1024,2048]{1,0:T(8,128)(2,1)} async-done(((bf16[128,2048]{1,0:T(8,128)(2,1)}), bf16[1024,2048]{1,0:T(8,128)(2,1)}) %all-gather.4.cloned.1.call-update) | async-done | bytes 4194320 | tf_op jit(solution)/shard_map/all_gather | solution.py:192
  54.1 147.6 %all-gather.6.cloned.1.call-done = bf16[2048,1024]{1,0:T(8,128)(2,1)} async-done(((bf16[32,1024]{1,0:T(8,128)(2,1)}), bf16[2048,1024]{1,0:T(8,128)(2,1)}) %all-gather.6.cloned.1.call-update) | async-done | bytes 4194320 | tf_op jit(solution)/shard_map/all_gather | solution.py:21
  201.7 3.8 bitcast_reduce_fusion
  207.5 4.3 fusion.51
  211.9 1.6 reshape.141
  213.5 4.4 fusion.55
  217.9 2.7 tanh.8
  220.5 4.3 fusion.50
  224.9 2.6 reshape.142
  227.5 4.3 fusion.53
  231.8 2.0 reshape.139
  233.8 2.7 negate_add_fusion
  236.5 4.0 divide_multiply_fusion
  240.5 237.3 %while.12 = (s32[]{:T(128)}, f32[2,128,64]{1,2,0:T(8,128)S(1)}, f32[16,64,2,128]{3,1,0,2:T(8,128)S(1)}, f32[16,64,2,64]{3,2,1,0:T(2,128)}, bf16[16,64,2,64]{3,2,...) while((s32[]{:T(128)}, f32[2,128,64]{1,2,0:T(8,128)S(1)}, ...), condition=%wide.region_4.5_spmd, body=%wide.region_2.4_spmd.sunk | while | flops 32329792 | bytes 2025073 | solution.py:226
  241.4 1.2 bitcast_multiply_fusion.9
  244.1 9.8 %custom-call.8 = f32[2,1,64,64]{2,3,1,0:T(8,128)S(1)} custom-call(f32[2,1,64,64]{3,2,1,0:T(8,128)S(1)} %fusion.192), custom_call_target="InvertDiagBlocksLowerTriangular" | custom-call | tf_op jit(solution)/shard_map/while/body/eval_jaxpr/jit(_solve_triangular)/vmap()/triangular_solve | solution.py:132
  256.3 1.2 bitcast_multiply_fusion.9
  259.0 9.8 %custom-call.8 = f32[2,1,64,64]{2,3,1,0:T(8,128)S(1)} custom-call(f32[2,1,64,64]{3,2,1,0:T(8,128)S(1)} %fusion.192), custom_call_target="InvertDiagBlocksLowerTriangular" | custom-call | tf_op jit(solution)/shard_map/while/body/eval_jaxpr/jit(_solve_triangular)/vmap()/triangular_solve | solution.py:132
  271.1 1.2 bitcast_multiply_fusion.9
  273.8 9.8 %custom-call.8 = f32[2,1,64,64]{2,3,1,0:T(8,128)S(1)} custom-call(f32[2,1,64,64]{3,2,1,0:T(8,128)S(1)} %fusion.192), custom_call_target="InvertDiagBlocksLowerTriangular" | custom-call | tf_op jit(solution)/shard_map/while/body/eval_jaxpr/jit(_solve_triangular)/vmap()/triangular_solve | solution.py:132
  285.9 1.2 bitcast_multiply_fusion.9
  288.6 9.9 %custom-call.8 = f32[2,1,64,64]{2,3,1,0:T(8,128)S(1)} custom-call(f32[2,1,64,64]{3,2,1,0:T(8,128)S(1)} %fusion.192), custom_call_target="InvertDiagBlocksLowerTriangular" | custom-call | tf_op jit(solution)/shard_map/while/body/eval_jaxpr/jit(_solve_triangular)/vmap()/triangular_solve | solution.py:132
  303.5 9.9 %custom-call.8 = f32[2,1,64,64]{2,3,1,0:T(8,128)S(1)} custom-call(f32[2,1,64,64]{3,2,1,0:T(8,128)S(1)} %fusion.192), custom_call_target="InvertDiagBlocksLowerTriangular" | custom-call | tf_op jit(solution)/shard_map/while/body/eval_jaxpr/jit(_solve_triangular)/vmap()/triangular_solve | solution.py:132
  318.3 9.8 %custom-call.8 = f32[2,1,64,64]{2,3,1,0:T(8,128)S(1)} custom-call(f32[2,1,64,64]{3,2,1,0:T(8,128)S(1)} %fusion.192), custom_call_target="InvertDiagBlocksLowerTriangular" | custom-call | tf_op jit(solution)/shard_map/while/body/eval_jaxpr/jit(_solve_triangular)/vmap()/triangular_solve | solution.py:132
  333.1 9.8 %custom-call.8 = f32[2,1,64,64]{2,3,1,0:T(8,128)S(1)} custom-call(f32[2,1,64,64]{3,2,1,0:T(8,128)S(1)} %fusion.192), custom_call_target="InvertDiagBlocksLowerTriangular" | custom-call | tf_op jit(solution)/shard_map/while/body/eval_jaxpr/jit(_solve_triangular)/vmap()/triangular_solve | solution.py:132
  347.9 9.8 %custom-call.8 = f32[2,1,64,64]{2,3,1,0:T(8,128)S(1)} custom-call(f32[2,1,64,64]{3,2,1,0:T(8,128)S(1)} %fusion.192), custom_call_target="InvertDiagBlocksLowerTriangular" | custom-call | tf_op jit(solution)/shard_map/while/body/eval_jaxpr/jit(_solve_triangular)/vmap()/triangular_solve | solution.py:132
  362.8 9.8 %custom-call.8 = f32[2,1,64,64]{2,3,1,0:T(8,128)S(1)} custom-call(f32[2,1,64,64]{3,2,1,0:T(8,128)S(1)} %fusion.192), custom_call_target="InvertDiagBlocksLowerTriangular" | custom-call | tf_op jit(solution)/shard_map/while/body/eval_jaxpr/jit(_solve_triangular)/vmap()/triangular_solve | solution.py:132
  374.9 1.2 bitcast_multiply_fusion.9
  377.6 9.8 %custom-call.8 = f32[2,1,64,64]{2,3,1,0:T(8,128)S(1)} custom-call(f32[2,1,64,64]{3,2,1,0:T(8,128)S(1)} %fusion.192), custom_call_target="InvertDiagBlocksLowerTriangular" | custom-call | tf_op jit(solution)/shard_map/while/body/eval_jaxpr/jit(_solve_triangular)/vmap()/triangular_solve | solution.py:132
  392.4 9.8 %custom-call.8 = f32[2,1,64,64]{2,3,1,0:T(8,128)S(1)} custom-call(f32[2,1,64,64]{3,2,1,0:T(8,128)S(1)} %fusion.192), custom_call_target="InvertDiagBlocksLowerTriangular" | custom-call | tf_op jit(solution)/shard_map/while/body/eval_jaxpr/jit(_solve_triangular)/vmap()/triangular_solve | solution.py:132
  407.3 9.8 %custom-call.8 = f32[2,1,64,64]{2,3,1,0:T(8,128)S(1)} custom-call(f32[2,1,64,64]{3,2,1,0:T(8,128)S(1)} %fusion.192), custom_call_target="InvertDiagBlocksLowerTriangular" | custom-call | tf_op jit(solution)/shard_map/while/body/eval_jaxpr/jit(_solve_triangular)/vmap()/triangular_solve | solution.py:132
  419.4 1.2 bitcast_multiply_fusion.9
  422.1 9.8 %custom-call.8 = f32[2,1,64,64]{2,3,1,0:T(8,128)S(1)} custom-call(f32[2,1,64,64]{3,2,1,0:T(8,128)S(1)} %fusion.192), custom_call_target="InvertDiagBlocksLowerTriangular" | custom-call | tf_op jit(solution)/shard_map/while/body/eval_jaxpr/jit(_solve_triangular)/vmap()/triangular_solve | solution.py:132
  436.9 9.8 %custom-call.8 = f32[2,1,64,64]{2,3,1,0:T(8,128)S(1)} custom-call(f32[2,1,64,64]{3,2,1,0:T(8,128)S(1)} %fusion.192), custom_call_target="InvertDiagBlocksLowerTriangular" | custom-call | tf_op jit(solution)/shard_map/while/body/eval_jaxpr/jit(_solve_triangular)/vmap()/triangular_solve | solution.py:132
  451.7 9.8 %custom-call.8 = f32[2,1,64,64]{2,3,1,0:T(8,128)S(1)} custom-call(f32[2,1,64,64]{3,2,1,0:T(8,128)S(1)} %fusion.192), custom_call_target="InvertDiagBlocksLowerTriangular" | custom-call | tf_op jit(solution)/shard_map/while/body/eval_jaxpr/jit(_solve_triangular)/vmap()/triangular_solve | solution.py:132
  463.9 1.2 bitcast_multiply_fusion.9
  466.6 9.8 %custom-call.8 = f32[2,1,64,64]{2,3,1,0:T(8,128)S(1)} custom-call(f32[2,1,64,64]{3,2,1,0:T(8,128)S(1)} %fusion.192), custom_call_target="InvertDiagBlocksLowerTriangular" | custom-call | tf_op jit(solution)/shard_map/while/body/eval_jaxpr/jit(_solve_triangular)/vmap()/triangular_solve | solution.py:132
  479.0 7.5 %all-to-all-start = ((bf16[16,256,64]{1,2,0:T(8,128)(2,1)}), bf16[16,256,64]{1,2,0:T(8,128)(2,1)S(1)}, u32[]{:S(2)}, u32[]{:S(2)}) async-start(bf16[16,256,64]{1,2,0:T(8,128)(2,1)} %broadcast_in_dim.79), calls=%async_computation | async-start | bytes 1048576 | tf_op jit(solution)/shard_map/all_to_all | solution.py:27
  486.8 3.7 fusion.58
  490.5 2.3 fusion.57
  492.9 3.8 collective-permute-start
  498.0 10.0 %fusion.79 = f32[1024,2048]{1,0:T(8,128)} fusion(bf16[2048,256]{1,0:T(8,128)(2,1)} %all-gather.8.cloned.1.call-done, f32[2,128]{1,0:T(2,128)S(1)} %collective-permute-done, f32[1024,128]{1,0:T(8,128)S(1)} %fusion.57, bf16[1024,2048]{1,0:T(8,128)(2,1)} %all-gather.4.cloned.1.call-done, bf16[2048,1024]{1,0:T(8,128)(2,1)} %all-gather.6.cloned.1.call-done, ...), kind=kOutput, calls=%fused_computation.125 | convolution fusion | flops 1075183616 | bytes 14158336 | tf_op jit(solution)/shard_map/dot_general | solution.py:260
  511.1 6.8 %add_convert_fusion = bf16[1024,2048]{1,0:T(8,128)(2,1)} fusion(f32[1024,2048]{1,0:T(8,128)} %fusion.79, bf16[1024,128]{0,1:T(8,128)(2,1)S(1)} %bitcast.179, bf16[2048,256]{1,0:T(8,128)(2,1)} %all-gather.8.cloned.1.call-done), kind=kOutput, calls=%fused_computation.74 | convolution fusion | flops 541065216 | bytes 13369344 | tf_op jit(solution)/shard_map/dot_general | solution.py:261
  517.9 49.1 %reduce-scatter.2.cloned.1.call-done = bf16[128,2048]{1,0:T(8,128)(2,1)} async-done(((bf16[1024,2048]{1,0:T(8,128)(2,1)}), bf16[128,2048]{1,0:T(8,128)(2,1)}) %reduce-scatter.2.cloned.1.call-update) | async-done | bytes 524304 | tf_op jit(solution)/shard_map/reduce_scatter | solution.py:258
  (370 shorter events, 85.6 us)
Async XLA Ops:
  6.5 503.9 %copy-start = (f32[1,2,64,64]{3,2,1,0:T(8,128)S(1)}, f32[1,2,64,64]{3,2,1,0:T(8,128)}, u32[]{:S(2)}) copy-start(f32[1,2,64,64]{3,2,1,0:T(8,128)} %param.34) | copy-start | bytes 98308
  6.5 47.6 %all-gather.4.cloned.1.call-start = ((), (), s32[]{:S(2)}) async-start(), calls=%async_computation.2 | async-start | bytes 4718592 | tf_op jit(solution)/shard_map/all_gather | solution.py:192
  9.9 191.9 %all-gather.6.cloned.1.call-start = ((), (), s32[]{:S(2)}) async-start(), calls=%async_computation.3 | async-start | bytes 4259840 | tf_op jit(solution)/shard_map/all_gather | solution.py:21
  15.5 0.6 copy-start.2
  16.2 480.9 %all-gather.8.cloned.1.call-start = ((), (), s32[]{:S(2)}) async-start(), calls=%async_computation.4 | async-start | bytes 1064960 | tf_op jit(solution)/shard_map/all_gather | solution.py:76
  240.5 246.3 %copy-start.3 = (f32[3,128]{1,0:T(4,128)S(1)}, f32[3,128]{1,0:T(4,128)}, u32[]{:S(2)}) copy-start(f32[3,128]{1,0:T(4,128)} %param.25) | copy-start | bytes 4612
  479.0 29.0 %all-to-all-start = ((bf16[16,256,64]{1,2,0:T(8,128)(2,1)}), bf16[16,256,64]{1,2,0:T(8,128)(2,1)S(1)}, u32[]{:S(2)}, u32[]{:S(2)}) async-start(bf16[16,256,64]{1,2,0:T(8,128)(2,1)} %broadcast_in_dim.79), calls=%async_computation | async-start | bytes 1048576 | tf_op jit(solution)/shard_map/all_to_all | solution.py:27
  486.6 80.5 %reduce-scatter.2.cloned.1.call-start = ((), (), s32[]{:S(2)}) async-start(), calls=%async_computation.5 | async-start | bytes 4718592 | tf_op jit(solution)/shard_map/reduce_scatter | solution.py:258
  486.8 3.7 copy-start.1
  490.5 6.2 %copy-start.4 = (f32[128]{0:T(128)S(1)}, f32[128]{0:T(128)}, u32[]{:S(2)}) copy-start(f32[128]{0:T(128)} %param.35) | copy-start | bytes 1540
  492.9 5.1 collective-permute-start
Sparse Core Ops, SparseCore 0:
  10.0 44.0 all-gather.3
  57.0 144.6 all-gather.5
  204.7 136.9 all-gather.7
  518.1 48.9 reduce-scatter.1
where the time goes:
time: 577 us; the launch traced here: 574 us
  waiting for transfers between devices  230 us (40%)
  other arithmetic  205 us (36%)
  matrix products  75.6 us (13%)
  local copies, waits for them, and re-layouts  36.4 us (6%)
  between operations  13.5 us (2%)
  starting transfers between devices  11.7 us (2%)
    another operation x32, other arithmetic, block_pass(): jax.scipy.linalg.solve_triangular(system, right_side, lower=True, unit_di...  157 us
    all_gather x1, waiting for transfers between devices, side_by_side(): out = lax.all_gather(both, axis, axis=dim, tiled=True)  148 us
    reduce_scatter x1, waiting for transfers between devices, on_device(): lax.psum_scatter((jnp.dot(conv_mixed, conv_whole, preferred_element_type=...  49.1 us
    all_gather x1, waiting for transfers between devices, on_device(): piece = lax.all_gather(normed, 'tp', axis=0, tiled=True)  32.2 us
    dot_general x7, matrix products, project(): jnp.dot(activations, weight, preferred_element_type=jnp.float32)  27.1 us
    mul x16, other arithmetic, block_pass(): ask_reads = queries * jnp.exp(cumulative - middle)  19.7 us
    another operation x16, other arithmetic, block_pass(): cumulative = jnp.cumsum(logarithm_decay, axis=0)  14.6 us
    dynamic_slice x32, local copies, waits for them, and re-layouts, on_device(): lax.scan(block_pass, initial_rows, tuple((in_blocks(array) for array in (...  12.7 us
  transfers between devices with their start and end apart: 6, of which 4 were waited for; matrix products, arithmetic and copies ran while one was open for 53% of the time, Pallas kernels for 0%

commit v1 on v0

--- a/solution.py
+++ b/solution.py
@@ -7,6 +7,14 @@
 BLOCK = 64
 norm_eps = 1e-06
 key_eps = 1e-06
+
+
+def gather_by_exchange(shard, axis, dim):
+    peers = lax.axis_size(axis)
+    repeats = [peers if d == dim else 1 for d in range(shard.ndim)]
+    return lax.all_to_all(
+        jnp.tile(shard, repeats), axis, split_axis=dim, concat_axis=dim, tiled=True
+    )
 
 
 def passed_along(block, axis, distance):
@@ -189,7 +197,7 @@
         0,
         1,
     )
-    piece = lax.all_gather(normed, "tp", axis=0, tiled=True)
+    piece = gather_by_exchange(normed, "tp", 0)
     projected = jnp.concatenate([project(piece, weight) for weight in gathered], axis=1)
     pieces = jnp.split(projected, 8, axis=1)
     conv_mixed = conv_branch(pieces[0], pieces[1], pieces[2], convolution_taps)

time: 577 us -> 537 us (0.931)
  waiting for transfers between devices: 230 us -> 186 us
    all_gather x1, waiting for transfers between devices: 148 us -> 89.7 us  [side_by_side(): out = lax.all_gather(both, axis, axis=dim, tiled=True)]
    all_to_all x0 -> x1, waiting for transfers between devices: none -> 46.9 us  [gather_by_exchange(): lax.all_to_all(jnp.tile(shard, repeats), axis, split_axis=dim, concat_axi...]
    all_gather x1 -> x0, waiting for transfers between devices: 32.2 us -> none  [on_device(): piece = lax.all_gather(normed, 'tp', axis=0, tiled=True)]
  transfers between devices with their start and end apart: 6 -> 6, of which waited for: 4 -> 4; matrix products, arithmetic and copies ran while one was open for 53% -> 56% of each run, Pallas kernels for 0% -> 0%
where the time goes in v1:
time: 537 us; the launch traced here: 534 us
  other arithmetic  204 us (38%)
  waiting for transfers between devices  186 us (35%)
  matrix products  76.8 us (14%)
  local copies, waits for them, and re-layouts  36.6 us (7%)
  starting transfers between devices  16.2 us (3%)
  between operations  13.5 us (3%)
    another operation x32, other arithmetic, block_pass(): jax.scipy.linalg.solve_triangular(system, right_side, lower=True, unit_di...  157 us
    all_gather x1, waiting for transfers between devices, side_by_side(): out = lax.all_gather(both, axis, axis=dim, tiled=True)  89.7 us
    reduce_scatter x1, waiting for transfers between devices, on_device(): lax.psum_scatter((jnp.dot(conv_mixed, conv_whole, preferred_element_type=...  48.2 us
    all_to_all x1, waiting for transfers between devices, gather_by_exchange(): lax.all_to_all(jnp.tile(shard, repeats), axis, split_axis=dim, concat_axi...  46.9 us
    dot_general x7, matrix products, project(): jnp.dot(activations, weight, preferred_element_type=jnp.float32)  28.3 us
    mul x16, other arithmetic, block_pass(): ask_reads = queries * jnp.exp(cumulative - middle)  19.7 us
    another operation x16, other arithmetic, block_pass(): cumulative = jnp.cumsum(logarithm_decay, axis=0)  14.6 us
    dynamic_slice x32, local copies, waits for them, and re-layouts, on_device(): lax.scan(block_pass, initial_rows, tuple((in_blocks(array) for array in (...  12.7 us
  transfers between devices with their start and end apart: 6, of which 4 were waited for; matrix products, arithmetic and copies ran while one was open for 56% of the time, Pallas kernels for 0%

profile of v1, /device:TPU:8, one launch (start us, length us, event | category | flops | bytes accessed | tf_op | source)
XLA Modules:
  0.0 533.9 jit_solution(17773656821805206523)
XLA Ops:
  14.1 1.2 fusion.65
  15.3 2.5 tile.2
  17.9 4.7 all-to-all-start
  23.5 1.6 reshape_squeeze.3
  25.3 46.9 %all-to-all-done = bf16[8,128,2048]{2,1,0:T(8,128)(2,1)} async-done(((bf16[8,128,2048]{2,1,0:T(8,128)(2,1)}), bf16[8,128,2048]{2,1,0:T(8,128)(2,1)}, u32[]{:S(2)}, u32[]{:S(2)}) %all-to-all-start) | async-done | bytes 4194336 | tf_op jit(solution)/shard_map/all_to_all | solution.py:15
  72.2 89.7 %all-gather.3.cloned.1.call-done = bf16[2048,1024]{1,0:T(8,128)(2,1)} async-done(((bf16[32,1024]{1,0:T(8,128)(2,1)}), bf16[2048,1024]{1,0:T(8,128)(2,1)}) %all-gather.3.cloned.1.call-update) | async-done | bytes 4194320 | tf_op jit(solution)/shard_map/all_gather | solution.py:29
  161.9 3.8 bitcast_reduce_fusion
  167.8 4.3 fusion.51
  172.1 1.6 reshape.179
  173.8 4.4 fusion.55
  178.1 2.6 tanh.8
  180.8 4.3 fusion.50
  185.1 2.6 reshape.180
  187.7 4.3 fusion.53
  192.0 2.0 reshape.177
  194.0 2.7 negate_add_fusion
  196.7 4.0 divide_multiply_fusion
  200.8 237.3 %while.12 = (s32[]{:T(128)}, f32[2,128,64]{1,2,0:T(8,128)S(1)}, f32[16,64,2,128]{3,1,0,2:T(8,128)S(1)}, f32[16,64,2,64]{3,2,1,0:T(2,128)}, bf16[16,64,2,64]{3,2,...) while((s32[]{:T(128)}, f32[2,128,64]{1,2,0:T(8,128)S(1)}, ...), condition=%wide.region_4.5_spmd, body=%wide.region_2.4_spmd.sunk | while | flops 32329792 | bytes 2025073 | solution.py:234
  201.7 1.2 bitcast_multiply_fusion.9
  204.4 9.8 %custom-call.8 = f32[2,1,64,64]{2,3,1,0:T(8,128)S(1)} custom-call(f32[2,1,64,64]{3,2,1,0:T(8,128)S(1)} %fusion.192), custom_call_target="InvertDiagBlocksLowerTriangular" | custom-call | tf_op jit(solution)/shard_map/while/body/eval_jaxpr/jit(_solve_triangular)/vmap()/triangular_solve | solution.py:140
  216.5 1.2 bitcast_multiply_fusion.9
  219.2 9.8 %custom-call.8 = f32[2,1,64,64]{2,3,1,0:T(8,128)S(1)} custom-call(f32[2,1,64,64]{3,2,1,0:T(8,128)S(1)} %fusion.192), custom_call_target="InvertDiagBlocksLowerTriangular" | custom-call | tf_op jit(solution)/shard_map/while/body/eval_jaxpr/jit(_solve_triangular)/vmap()/triangular_solve | solution.py:140
  231.3 1.2 bitcast_multiply_fusion.9
  234.0 9.8 %custom-call.8 = f32[2,1,64,64]{2,3,1,0:T(8,128)S(1)} custom-call(f32[2,1,64,64]{3,2,1,0:T(8,128)S(1)} %fusion.192), custom_call_target="InvertDiagBlocksLowerTriangular" | custom-call | tf_op jit(solution)/shard_map/while/body/eval_jaxpr/jit(_solve_triangular)/vmap()/triangular_solve | solution.py:140
  246.2 1.3 bitcast_multiply_fusion.9
  248.9 9.9 %custom-call.8 = f32[2,1,64,64]{2,3,1,0:T(8,128)S(1)} custom-call(f32[2,1,64,64]{3,2,1,0:T(8,128)S(1)} %fusion.192), custom_call_target="InvertDiagBlocksLowerTriangular" | custom-call | tf_op jit(solution)/shard_map/while/body/eval_jaxpr/jit(_solve_triangular)/vmap()/triangular_solve | solution.py:140
  263.7 9.9 %custom-call.8 = f32[2,1,64,64]{2,3,1,0:T(8,128)S(1)} custom-call(f32[2,1,64,64]{3,2,1,0:T(8,128)S(1)} %fusion.192), custom_call_target="InvertDiagBlocksLowerTriangular" | custom-call | tf_op jit(solution)/shard_map/while/body/eval_jaxpr/jit(_solve_triangular)/vmap()/triangular_solve | solution.py:140
  275.8 1.2 bitcast_multiply_fusion.9
  278.5 9.8 %custom-call.8 = f32[2,1,64,64]{2,3,1,0:T(8,128)S(1)} custom-call(f32[2,1,64,64]{3,2,1,0:T(8,128)S(1)} %fusion.192), custom_call_target="InvertDiagBlocksLowerTriangular" | custom-call | tf_op jit(solution)/shard_map/while/body/eval_jaxpr/jit(_solve_triangular)/vmap()/triangular_solve | solution.py:140
  293.4 9.8 %custom-call.8 = f32[2,1,64,64]{2,3,1,0:T(8,128)S(1)} custom-call(f32[2,1,64,64]{3,2,1,0:T(8,128)S(1)} %fusion.192), custom_call_target="InvertDiagBlocksLowerTriangular" | custom-call | tf_op jit(solution)/shard_map/while/body/eval_jaxpr/jit(_solve_triangular)/vmap()/triangular_solve | solution.py:140
  308.2 9.8 %custom-call.8 = f32[2,1,64,64]{2,3,1,0:T(8,128)S(1)} custom-call(f32[2,1,64,64]{3,2,1,0:T(8,128)S(1)} %fusion.192), custom_call_target="InvertDiagBlocksLowerTriangular" | custom-call | tf_op jit(solution)/shard_map/while/body/eval_jaxpr/jit(_solve_triangular)/vmap()/triangular_solve | solution.py:140
  323.0 9.8 %custom-call.8 = f32[2,1,64,64]{2,3,1,0:T(8,128)S(1)} custom-call(f32[2,1,64,64]{3,2,1,0:T(8,128)S(1)} %fusion.192), custom_call_target="InvertDiagBlocksLowerTriangular" | custom-call | tf_op jit(solution)/shard_map/while/body/eval_jaxpr/jit(_solve_triangular)/vmap()/triangular_solve | solution.py:140
  337.9 9.8 %custom-call.8 = f32[2,1,64,64]{2,3,1,0:T(8,128)S(1)} custom-call(f32[2,1,64,64]{3,2,1,0:T(8,128)S(1)} %fusion.192), custom_call_target="InvertDiagBlocksLowerTriangular" | custom-call | tf_op jit(solution)/shard_map/while/body/eval_jaxpr/jit(_solve_triangular)/vmap()/triangular_solve | solution.py:140
  352.7 9.8 %custom-call.8 = f32[2,1,64,64]{2,3,1,0:T(8,128)S(1)} custom-call(f32[2,1,64,64]{3,2,1,0:T(8,128)S(1)} %fusion.192), custom_call_target="InvertDiagBlocksLowerTriangular" | custom-call | tf_op jit(solution)/shard_map/while/body/eval_jaxpr/jit(_solve_triangular)/vmap()/triangular_solve | solution.py:140
  364.8 1.2 bitcast_multiply_fusion.9
  367.5 9.8 %custom-call.8 = f32[2,1,64,64]{2,3,1,0:T(8,128)S(1)} custom-call(f32[2,1,64,64]{3,2,1,0:T(8,128)S(1)} %fusion.192), custom_call_target="InvertDiagBlocksLowerTriangular" | custom-call | tf_op jit(solution)/shard_map/while/body/eval_jaxpr/jit(_solve_triangular)/vmap()/triangular_solve | solution.py:140
  382.3 9.8 %custom-call.8 = f32[2,1,64,64]{2,3,1,0:T(8,128)S(1)} custom-call(f32[2,1,64,64]{3,2,1,0:T(8,128)S(1)} %fusion.192), custom_call_target="InvertDiagBlocksLowerTriangular" | custom-call | tf_op jit(solution)/shard_map/while/body/eval_jaxpr/jit(_solve_triangular)/vmap()/triangular_solve | solution.py:140
  397.2 9.8 %custom-call.8 = f32[2,1,64,64]{2,3,1,0:T(8,128)S(1)} custom-call(f32[2,1,64,64]{3,2,1,0:T(8,128)S(1)} %fusion.192), custom_call_target="InvertDiagBlocksLowerTriangular" | custom-call | tf_op jit(solution)/shard_map/while/body/eval_jaxpr/jit(_solve_triangular)/vmap()/triangular_solve | solution.py:140
  409.3 1.2 bitcast_multiply_fusion.9
  412.0 9.8 %custom-call.8 = f32[2,1,64,64]{2,3,1,0:T(8,128)S(1)} custom-call(f32[2,1,64,64]{3,2,1,0:T(8,128)S(1)} %fusion.192), custom_call_target="InvertDiagBlocksLowerTriangular" | custom-call | tf_op jit(solution)/shard_map/while/body/eval_jaxpr/jit(_solve_triangular)/vmap()/triangular_solve | solution.py:140
  426.8 9.8 %custom-call.8 = f32[2,1,64,64]{2,3,1,0:T(8,128)S(1)} custom-call(f32[2,1,64,64]{3,2,1,0:T(8,128)S(1)} %fusion.192), custom_call_target="InvertDiagBlocksLowerTriangular" | custom-call | tf_op jit(solution)/shard_map/while/body/eval_jaxpr/jit(_solve_triangular)/vmap()/triangular_solve | solution.py:140
  439.3 7.5 %all-to-all-start.1 = ((bf16[16,256,64]{1,2,0:T(8,128)(2,1)}), bf16[16,256,64]{1,2,0:T(8,128)(2,1)S(1)}, u32[]{:S(2)}, u32[]{:S(2)}) async-start(bf16[16,256,64]{1,2,0:T(8,128)(2,1)} %broadcast_in_dim.79), calls=%async_computation.1 | async-start | bytes 1048576 | tf_op jit(solution)/shard_map/all_to_all | solution.py:35
  446.9 3.5 fusion.58
  450.4 3.6 fusion.57
  454.0 3.8 collective-permute-start
  459.1 10.1 %fusion.79 = f32[1024,2048]{1,0:T(8,128)} fusion(bf16[2048,256]{1,0:T(8,128)(2,1)} %all-gather.5.cloned.1.call-done, f32[2,128]{1,0:T(2,128)S(1)} %collective-permute-done, f32[1024,128]{1,0:T(8,128)S(1)} %fusion.57, bf16[1024,2048]{1,0:T(8,128)(2,1)} %bitcast.16, bf16[2048,1024]{1,0:T(8,128)(2,1)} %all-gather.3.cloned.1.call-done, ...), kind=kOutput, calls=%fused_computation.125 | convolution fusion | flops 1075183616 | bytes 14158336 | tf_op jit(solution)/shard_map/dot_general | solution.py:268
  472.3 6.8 %add_convert_fusion = bf16[1024,2048]{1,0:T(8,128)(2,1)} fusion(f32[1024,2048]{1,0:T(8,128)} %fusion.79, bf16[1024,128]{0,1:T(8,128)(2,1)S(1)} %bitcast.180, bf16[2048,256]{1,0:T(8,128)(2,1)} %all-gather.5.cloned.1.call-done), kind=kOutput, calls=%fused_computation.74 | convolution fusion | flops 541065216 | bytes 13369344 | tf_op jit(solution)/shard_map/dot_general | solution.py:269
  479.1 48.2 %reduce-scatter.2.cloned.1.call-done = bf16[128,2048]{1,0:T(8,128)(2,1)} async-done(((bf16[1024,2048]{1,0:T(8,128)(2,1)}), bf16[128,2048]{1,0:T(8,128)(2,1)}) %reduce-scatter.2.cloned.1.call-update) | async-done | bytes 524304 | tf_op jit(solution)/shard_map/reduce_scatter | solution.py:266
  (378 shorter events, 86.1 us)
Async XLA Ops:
  6.5 465.1 %copy-start = (f32[1,2,64,64]{3,2,1,0:T(8,128)S(1)}, f32[1,2,64,64]{3,2,1,0:T(8,128)}, u32[]{:S(2)}) copy-start(f32[1,2,64,64]{3,2,1,0:T(8,128)} %param.34) | copy-start | bytes 98308
  6.5 155.4 %all-gather.3.cloned.1.call-start = ((), (), s32[]{:S(2)}) async-start(), calls=%async_computation.3 | async-start | bytes 4259840 | tf_op jit(solution)/shard_map/all_gather | solution.py:29
  12.2 0.6 copy-start.2
  17.8 4.8 copy-start.3
  17.8 4.8 copy-start.4
  17.8 5.5 %copy-start.6 = (f32[128]{0:T(128)S(1)}, f32[128]{0:T(128)}, u32[]{:S(2)}) copy-start(f32[128]{0:T(128)} %param.32) | copy-start | bytes 1540
  17.8 5.6 %copy-start.1 = (f32[1,1024,128]{2,1,0:T(8,128)S(1)}, f32[1,1024,128]{2,1,0:T(8,128)}, u32[]{:S(2)}) copy-start(f32[1,1024,128]{2,1,0:T(8,128)} %param.33) | copy-start | bytes 1572868
  17.8 7.2 %copy-start.7 = (f32[128]{0:T(128)S(1)}, f32[128]{0:T(128)}, u32[]{:S(2)}) copy-start(f32[128]{0:T(128)} %param.31) | copy-start | bytes 1540
  17.9 54.4 %all-to-all-start = ((bf16[8,128,2048]{2,1,0:T(8,128)(2,1)}), bf16[8,128,2048]{2,1,0:T(8,128)(2,1)}, u32[]{:S(2)}, u32[]{:S(2)}) async-start(bf16[8,128,2048]{2,1,0:T(8,128)(2,1)} %tile.2), calls=%async_computation | async-start | bytes 8388608 | tf_op jit(solution)/shard_map/all_to_all | solution.py:15
  22.6 435.7 %all-gather.5.cloned.1.call-start = ((), (), s32[]{:S(2)}) async-start(), calls=%async_computation.4 | async-start | bytes 1064960 | tf_op jit(solution)/shard_map/all_gather | solution.py:84
  200.7 246.1 %copy-start.5 = (f32[3,128]{1,0:T(4,128)S(1)}, f32[3,128]{1,0:T(4,128)}, u32[]{:S(2)}) copy-start(f32[3,128]{1,0:T(4,128)} %param.25) | copy-start | bytes 4612
  439.3 29.9 %all-to-all-start.1 = ((bf16[16,256,64]{1,2,0:T(8,128)(2,1)}), bf16[16,256,64]{1,2,0:T(8,128)(2,1)S(1)}, u32[]{:S(2)}, u32[]{:S(2)}) async-start(bf16[16,256,64]{1,2,0:T(8,128)(2,1)} %broadcast_in_dim.79), calls=%async_computation.1 | async-start | bytes 1048576 | tf_op jit(solution)/shard_map/all_to_all | solution.py:35
  446.8 80.5 %reduce-scatter.2.cloned.1.call-start = ((), (), s32[]{:S(2)}) async-start(), calls=%async_computation.5 | async-start | bytes 4718592 | tf_op jit(solution)/shard_map/reduce_scatter | solution.py:266
  450.4 7.4 %copy-start.8 = (f32[128]{0:T(128)S(1)}, f32[128]{0:T(128)}, u32[]{:S(2)}) copy-start(f32[128]{0:T(128)} %param.35) | copy-start | bytes 1540
  454.0 5.1 collective-permute-start
Sparse Core Ops, SparseCore 0:
  13.0 148.9 all-gather.2
  164.9 137.2 all-gather.4
  479.2 48.0 reduce-scatter.1
